TPU v7x, 128 devices: a whole 4x4x4 slice. The times are simulated.
128 devices in a mesh: ep: 16 (over z, x), tp: 8 (over y, core).
Axes of the slice: x: 4, y: 4, z: 4, core: 2. Of those that a mesh axis runs over, the one named last changes fastest.
Arguments:
- tokens: bfloat16 [16384, 2048], P(('ep', 'tp')), may hold values from -6 to 6
- expert_ids: int32 [16384, 4], P('ep'), may hold values from 0 to 15, all different within a row; in each aligned block of 128 rows (0 to 127, 128 to 255, ...) at most 64 rows name the same one
- gate_values: float32 [16384, 4], P('ep'), may hold values from 0.1 to 1
- norm_gain: float32 [2048], replicated, may hold values from 0.1 to 1.9
- gate_weight: bfloat16 [16, 2048, 1024], P('ep', None, 'tp'), may hold values from -0.125 to 0.125
- up_weight: bfloat16 [16, 2048, 1024], P('ep', None, 'tp'), may hold values from -0.125 to 0.125
- down_weight: bfloat16 [16, 1024, 2048], P('ep', 'tp'), may hold values from -0.1875 to 0.1875
- out_gain: float32 [2048], P('tp'), may hold values from 0.1 to 1.9
Outputs:
- mixed: bfloat16 [16384, 2048], P('ep', 'tp')
Inputs may be any that keep to these rules, and one draw needn't show every extreme that they name: `expert_ids`: each row names 4 different experts of 0 to 15; within the rows of one device (aligned blocks of 128 rows) no expert is named more than 64 times, and in some blocks one expert is named exactly 64 times.
All inputs are finite; a program needn't handle non-finite values.
Results may differ from a plain program's by a relative error of at most 0.0025.
Values may be sent and summed in bfloat16 or wider, within the bound.
No kernel may reach another device: no remote copies, remote signals or barrier semaphores. Data moves between devices by JAX's collectives and lax.ppermute only.
A program may use at most 64 MiB of HBM per device.

v0:
```python
import jax
import jax.numpy as jnp
from jax import lax
from jax.sharding import PartitionSpec as P

epsilon = 1e-05
clamp_limit = 7.0
sigmoid_alpha = 1.702


def taken_in(shard, axis, dim, absorb, state):
    everything = jax.tree.map(lambda a: lax.all_gather(a, axis, axis=dim, tiled=True), shard)
    return absorb(state, everything, jnp.int32(0))


def rms_rows(values, gain):
    mean_sq = jnp.mean(values * values, axis=-1, keepdims=True)
    return values * lax.rsqrt(mean_sq + epsilon) * gain


def clamped_unit(gate_part, up_part):
    glu_part = jnp.minimum(gate_part, clamp_limit)
    lin_part = jnp.clip(up_part, -clamp_limit, clamp_limit)
    return glu_part * jax.nn.sigmoid(sigmoid_alpha * glu_part) * (lin_part + 1.0)


def local(
    tokens, expert_ids, gate_values, norm_gain, gate_weight, up_weight, down_weight, out_gain
):
    expert_groups = lax.axis_size("ep")
    width_groups = lax.axis_size("tp")
    tok_rows = tokens.shape[0]
    model_width = tokens.shape[1]
    top_count = expert_ids.shape[1]
    capacity = tok_rows // 2
    per_rank = capacity // width_groups
    slice_w = model_width // width_groups
    normed = rms_rows(tokens.astype(jnp.float32), norm_gain).astype(jnp.bfloat16)
    blocks = expert_ids.reshape(width_groups, tok_rows * top_count)
    onehot = (
        blocks[:, :, None] == jnp.arange(expert_groups, dtype=jnp.int32)[None, None, :]
    ).astype(jnp.int32)
    slot_num = jnp.sum((jnp.cumsum(onehot, axis=1) - onehot) * onehot, axis=2)
    own_rank = lax.axis_index("tp")
    own_ids = lax.dynamic_index_in_dim(blocks, own_rank, 0, keepdims=False)
    own_slots = lax.dynamic_index_in_dim(slot_num, own_rank, 0, keepdims=False)
    target = own_ids * capacity + own_slots
    entry_token = jnp.arange(tok_rows * top_count, dtype=jnp.int32) // top_count
    owner_row = (
        jnp.full((expert_groups * capacity,), tok_rows, jnp.int32).at[target].set(entry_token)
    )
    padded = jnp.concatenate([normed, jnp.zeros((1, model_width), jnp.bfloat16)], axis=0)
    outgoing = padded[owner_row].reshape(expert_groups * width_groups, per_rank, model_width)
    arrived = lax.all_to_all(outgoing, ("ep", "tp"), split_axis=0, concat_axis=0, tiled=True)
    arrived_rows = arrived.reshape(-1, model_width)
    row_total = arrived_rows.shape[0]
    hidden_width = gate_weight.shape[2] * width_groups
    blank_acts = jnp.zeros((row_total, hidden_width), jnp.bfloat16)

    def add_hidden(activated, pieces, offset):
        gate_part = jnp.dot(arrived_rows, pieces[0][0], preferred_element_type=jnp.float32)
        up_part = jnp.dot(arrived_rows, pieces[1][0], preferred_element_type=jnp.float32)
        fresh = clamped_unit(gate_part, up_part).astype(jnp.bfloat16)
        return lax.dynamic_update_slice_in_dim(activated, fresh, offset, 1)

    activated = taken_in((gate_weight, up_weight), "tp", 2, add_hidden, blank_acts)

    def add_output(running, w_piece, offset):
        act_part = lax.dynamic_slice_in_dim(activated, offset, w_piece.shape[1], 1)
        return running + jnp.dot(act_part, w_piece[0], preferred_element_type=jnp.float32)

    blank_out = jnp.zeros((row_total, model_width), jnp.float32)
    result = taken_in(down_weight, "tp", 1, add_output, blank_out).astype(jnp.bfloat16)
    outbound = result.reshape(expert_groups, width_groups, per_rank, width_groups, slice_w)
    outbound = outbound.transpose(0, 3, 1, 2, 4)
    landed = lax.all_to_all(
        outbound.reshape(expert_groups * width_groups, width_groups, per_rank, slice_w),
        ("ep", "tp"),
        split_axis=0,
        concat_axis=0,
        tiled=True,
    )
    returned = landed.reshape(-1, slice_w)
    rank_part = slot_num // per_rank
    within = slot_num % per_rank
    source_col = jnp.arange(width_groups, dtype=jnp.int32)[:, None]
    row_index = (
        (blocks * width_groups + rank_part) * width_groups + source_col
    ) * per_rank + within
    picked = returned[row_index.reshape(-1)].astype(jnp.float32)
    picked = picked.reshape(width_groups * tok_rows, top_count, slice_w)
    combined = jnp.sum(gate_values[:, :, None] * picked, axis=1)
    local_sq = jnp.sum(combined * combined, axis=1)
    total_sq = lax.psum(local_sq, "tp")
    row_scale = lax.rsqrt(total_sq / model_width + epsilon)
    return (combined * row_scale[:, None] * out_gain).astype(jnp.bfloat16)


def solution(mesh):
    in_specs = (
        P(("ep", "tp"), None),
        P("ep", None),
        P("ep", None),
        P(),
        P("ep", None, "tp"),
        P("ep", None, "tp"),
        P("ep", "tp", None),
        P("tp"),
    )
    out_specs = P("ep", "tp")
    return jax.shard_map(local, mesh=mesh, in_specs=in_specs, out_specs=out_specs, check_vma=False)
```

profile of v0, /device:TPU:1, one launch (start us, length us, event | category | flops | bytes accessed | tf_op | source)
XLA Modules:
  0.0 281.1 jit_solution(7951599097116689879)
XLA Ops:
  6.5 0.0 copy-start
  6.5 0.0 copy-start.3
  6.5 0.0 all-gather.6.cloned.1.call-start
  6.5 0.7 all-gather.6.cloned.1.call-update
  7.3 0.0 all-gather.4.cloned.1.call-start
  7.3 0.7 all-gather.4.cloned.1.call-update
  8.0 0.0 all-gather.8.cloned.1.call-start
  8.1 0.7 all-gather.8.cloned.1.call-update
  8.7 0.9 copy.11
  9.7 0.3 eq.28
  10.0 0.3 reshape.220
  10.3 9.1 %reduce-window.6 = s32[8,16,4,128]{3,1,2,0:T(8,128)S(1)} reduce-window(s32[8,16,4,128]{3,1,2,0:T(8,128)S(1)} %fusion.21, s32[]{:T(128)} %constant.77.clone.1), window={size=1x1x1x128 pad=0_0x0_0x0_0x127_0}, to_apply=%region_1.0 | reduce-window | flops 8323072 | bytes 524292 | tf_op jit(solution)/shard_map/reduce-window
  19.4 0.1 slice.12
  19.5 0.3 copy.13
  19.8 0.1 fusion.23
  19.9 0.0 copy-done
  19.9 0.2 fusion.15
  20.1 0.0 copy-done.3
  20.1 0.2 fusion.17
  20.4 0.1 fusion.20
  20.6 2.4 scatter_custom_fusion
  23.0 6.0 %gather_fusion = bf16[1024,2048]{1,0:T(8,128)(2,1)} fusion(bf16[129,2048]{1,0:T(8,128)(2,1)S(1)} %concatenate.3, s32[1024]{0:T(1024)S(1)} %fusion.25), kind=kCustom, calls=%fused_computation | custom fusion | bytes 8392704 | tf_op jit(solution)/shard_map/gather | solution.py:53
  29.1 64.7 %all_to_all.10 = bf16[128,8,2048]{2,1,0:T(8,128)(2,1)} all-to-all(bf16[128,8,2048]{2,1,0:T(8,128)(2,1)} %bitcast.62), channel_id=1, replica_groups=mesh['ep'=16,'tp'=8] {'ep','tp'}, dimensions={0} | all-to-all | bytes 8388608 | tf_op jit(solution)/shard_map/all_to_all | solution.py:54
  93.7 0.0 all-gather.6.cloned.1.call-done
  93.7 9.9 %fusion.2 = f32[1024,1024]{1,0:T(8,128)} fusion(bf16[1,2048,1024]{2,1,0:T(8,128)(2,1)} %all-gather.6.cloned.1.call-done, bf16[128,8,2048]{2,1,0:T(8,128)(2,1)} %all_to_all.10), kind=kOutput, calls=%fused_computation.5 | convolution fusion | flops 4294967296 | bytes 12582912 | tf_op jit(solution)/shard_map/dot_general | solution.py:62
  103.6 26.1 %all-gather.4.cloned.1.call-done = bf16[1,2048,1024]{2,1,0:T(8,128)(2,1)} async-done(((bf16[1,2048,128]{2,1,0:T(8,128)(2,1)}), bf16[1,2048,1024]{2,1,0:T(8,128)(2,1)}) %all-gather.4.cloned.1.call-update) | async-done | bytes 4194320 | tf_op jit(solution)/shard_map/all_gather | solution.py:12
  129.7 10.1 %multiply_convert_fusion = bf16[1024,1024]{1,0:T(8,128)(2,1)S(1)} fusion(f32[1024,1024]{1,0:T(8,128)} %fusion.2, bf16[1,2048,1024]{2,1,0:T(8,128)(2,1)} %all-gather.4.cloned.1.call-done, bf16[128,8,2048]{2,1,0:T(8,128)(2,1)} %all_to_all.10), kind=kOutput, calls=%fused_computation.12 | convolution fusion | flops 4305453056 | bytes 14680064 | tf_op jit(solution)/shard_map/dot_general | solution.py:61
  139.8 24.7 %all-gather.8.cloned.1.call-done = bf16[1,1024,2048]{2,1,0:T(8,128)(2,1)} async-done(((bf16[1,128,2048]{2,1,0:T(8,128)(2,1)}), bf16[1,1024,2048]{2,1,0:T(8,128)(2,1)}) %all-gather.8.cloned.1.call-update) | async-done | bytes 4194320 | tf_op jit(solution)/shard_map/all_gather | solution.py:12
  164.5 6.9 %fusion.8 = bf16[1024,2048]{1,0:T(8,128)(2,1)S(1)} fusion(bf16[1024,1024]{1,0:T(8,128)(2,1)S(1)} %multiply_convert_fusion, bf16[1,1024,2048]{2,1,0:T(8,128)(2,1)} %all-gather.8.cloned.1.call-done), kind=kOutput, calls=%fused_computation.13 | convolution fusion | flops 4297064448 | bytes 10485760 | tf_op jit(solution)/shard_map/dot_general | solution.py:70
  171.3 2.6 copy.16
  173.9 0.0 copy-start.1
  173.9 0.0 copy-start.2
  173.9 8.3 %all-to-all-start.1 = ((bf16[128,8,8,256]{3,2,1,0:T(8,128)(2,1)}), bf16[128,8,8,256]{3,2,1,0:T(8,128)(2,1)}, u32[]{:S(2)}, u32[]{:S(2)}) async-start(bf16[128,8,8,256]{3,2,1,0:T(8,128)(2,1)} %bitcast.63), calls=%async_computation.1 | async-start | bytes 8388608 | tf_op jit(solution)/shard_map/all_to_all | solution.py:76
  182.2 0.0 copy-done.1
  182.3 0.2 copy.17
  182.5 0.3 mul.125
  182.9 0.0 copy-done.2
  182.9 0.2 copy.10
  183.1 0.2 compare_select_fusion
  183.3 51.6 %all-to-all-done.1 = bf16[128,8,8,256]{3,2,1,0:T(8,128)(2,1)} async-done(((bf16[128,8,8,256]{3,2,1,0:T(8,128)(2,1)}), bf16[128,8,8,256]{3,2,1,0:T(8,128)(2,1)}, u32[]{:S(2)}, u32[]{:S(2)}) %all-to-all-start.1) | async-done | bytes 4194336 | tf_op jit(solution)/shard_map/all_to_all | solution.py:76
  234.9 15.7 %gather_fusion.1 = bf16[4096,256]{1,0:T(8,128)(2,1)S(1)} fusion(bf16[8192,256]{1,0:T(8,128)(2,1)} %bitcast.12, s32[4096]{0:T(1024)S(1)} %broadcast_clamp_fusion), kind=kCustom, calls=%fused_computation.1 | custom fusion | bytes 4210688 | tf_op jit(solution)/shard_map/gather | solution.py:90
  250.6 2.9 %reshape.227 = f32[1024,4,256]{2,1,0:T(4,128)} reshape(bf16[4096,256]{1,0:T(8,128)(2,1)S(1)} %gather_fusion.1) | data formatting | bytes 6291456 | tf_op jit(solution)/shard_map/convert_element_type | solution.py:90
  253.5 0.0 copy-start.4
  253.5 7.2 %multiply_reduce_fusion = f32[1024,256]{1,0:T(8,128)S(1)} fusion(f32[1024,4,256]{2,1,0:T(4,128)} %reshape.227, f32[1024,4]{1,0:T(8,128)S(1)} %copy.10), kind=kLoop, calls=%fused_computation.11 | loop fusion | flops 1835008 | bytes 5259264 | tf_op jit(solution)/shard_map/reduce_sum | solution.py:92
  260.7 0.2 multiply_reduce_fusion.1
  260.9 12.7 %psum.7 = f32[1024]{0:T(1024)S(1)} all-reduce(f32[1024]{0:T(1024)S(1)} %multiply_reduce_fusion.1), channel_id=1, replica_groups=mesh['ep'=16,'tp'=8] {'tp'}, use_global_device_ids=true, to_apply=%region_7.8 | all-reduce | flops 1024 | bytes 8192 | tf_op jit(solution)/shard_map/psum | solution.py:94
  273.6 0.0 copy-done.4
  273.6 1.0 multiply_convert_fusion.1
  (14 shorter events, 0.2 us)
Async XLA Ops:
  6.5 13.4 %copy-start = (bf16[128,2048]{1,0:T(8,128)(2,1)S(1)}, bf16[128,2048]{1,0:T(8,128)(2,1)}, u32[]{:S(2)}) copy-start(bf16[128,2048]{1,0:T(8,128)(2,1)} %param.8) | copy-start | bytes 1572868
  6.5 13.6 %copy-start.3 = (f32[2048]{0:T(1024)S(1)}, f32[2048]{0:T(1024)}, u32[]{:S(2)}) copy-start(f32[2048]{0:T(1024)} %param.11) | copy-start | bytes 24580
  6.5 87.2 %all-gather.6.cloned.1.call-start = ((), (), s32[]{:S(2)}) async-start(), calls=%async_computation.3 | async-start | bytes 4718592 | tf_op jit(solution)/shard_map/all_gather | solution.py:12
  7.3 122.5 %all-gather.4.cloned.1.call-start = ((), (), s32[]{:S(2)}) async-start(), calls=%async_computation.2 | async-start | bytes 4718592 | tf_op jit(solution)/shard_map/all_gather | solution.py:12
  8.0 156.4 %all-gather.8.cloned.1.call-start = ((), (), s32[]{:S(2)}) async-start(), calls=%async_computation.4 | async-start | bytes 4718592 | tf_op jit(solution)/shard_map/all_gather | solution.py:12
  173.9 8.3 %copy-start.1 = (s32[1024,4]{0,1:T(4,128)S(1)}, s32[1024,4]{0,1:T(4,128)}, u32[]{:S(2)}) copy-start(s32[1024,4]{0,1:T(4,128)} %param.9) | copy-start | bytes 49156
  173.9 9.0 %copy-start.2 = (f32[1024,4]{0,1:T(4,128)S(1)}, f32[1024,4]{0,1:T(4,128)}, u32[]{:S(2)}) copy-start(f32[1024,4]{0,1:T(4,128)} %param.10) | copy-start | bytes 49156
  173.9 61.0 %all-to-all-start.1 = ((bf16[128,8,8,256]{3,2,1,0:T(8,128)(2,1)}), bf16[128,8,8,256]{3,2,1,0:T(8,128)(2,1)}, u32[]{:S(2)}, u32[]{:S(2)}) async-start(bf16[128,8,8,256]{3,2,1,0:T(8,128)(2,1)} %bitcast.63), calls=%async_computation.1 | async-start | bytes 8388608 | tf_op jit(solution)/shard_map/all_to_all | solution.py:76
  253.5 20.1 %copy-start.4 = (f32[256]{0:T(256)S(1)}, f32[256]{0:T(256)}, u32[]{:S(2)}) copy-start(f32[256]{0:T(256)} %param.15) | copy-start | bytes 3076
Sparse Core Ops, SparseCore 0:
  9.0 63.1 all-gather.5
  73.9 55.8 all-gather.3
  131.4 32.9 all-gather.7
where the time goes:
time: 282 us; the launch traced here: 281 us
  waiting for transfers between devices  105 us (37%)
  blocking collectives  77.4 us (27%)
  local copies, waits for them, and re-layouts  32.4 us (11%)
  matrix products  26.8 us (10%)
  other arithmetic  18.3 us (6%)
  between operations  13.4 us (5%)
  starting transfers between devices  8.37 us (3%)
    all_to_all x1, blocking collectives, local(): lax.all_to_all(outgoing, ('ep', 'tp'), split_axis=0, concat_axis=0, tiled...  64.7 us
    all_to_all x1, waiting for transfers between devices, local(): lax.all_to_all(outbound.reshape(expert_groups * width_groups, width_group...  51.6 us
    all_gather x3, waiting for transfers between devices, taken_in(): lax.all_gather(a, axis, axis=dim, tiled=True)  50.8 us
    gather x1, local copies, waits for them, and re-layouts, local(): picked = returned[row_index.reshape(-1)].astype(jnp.float32)  15.7 us
    psum x1, blocking collectives, local(): total_sq = lax.psum(local_sq, 'tp')  12.7 us
    dot_general x1, matrix products, add_hidden(): jnp.dot(arrived_rows, pieces[0][0], preferred_element_type=jnp.float32)  10.1 us
    dot_general x1, matrix products, add_hidden(): jnp.dot(arrived_rows, pieces[1][0], preferred_element_type=jnp.float32)  9.88 us
    another operation x2, other arithmetic  9.2 us
  transfers between devices with their start and end apart: 4, of which 3 were waited for; matrix products, arithmetic and copies ran while one was open for 15% of the time, Pallas kernels for 0%

commit v1 on v0

--- a/solution.py
+++ b/solution.py
@@ -91,7 +91,9 @@
     picked = picked.reshape(width_groups * tok_rows, top_count, slice_w)
     combined = jnp.sum(gate_values[:, :, None] * picked, axis=1)
     local_sq = jnp.sum(combined * combined, axis=1)
-    total_sq = lax.psum(local_sq, "tp")
+    total_sq = local_sq
+    for hop in (1, 2, 4):
+        total_sq = total_sq + lax.ppermute(total_sq, "tp", [(dev, dev ^ hop) for dev in range(8)])
     row_scale = lax.rsqrt(total_sq / model_width + epsilon)
     return (combined * row_scale[:, None] * out_gain).astype(jnp.bfloat16)
 

time: 282 us -> 278 us (0.986)
  blocking collectives: 77.4 us -> 64.7 us
  waiting for transfers between devices: 105 us -> 111 us
    psum x1 -> x0, blocking collectives: 12.7 us -> none  [local(): total_sq = lax.psum(local_sq, 'tp')]
    ppermute x0 -> x3, waiting for transfers between devices: none -> 6.95 us  [local(): lax.ppermute(total_sq, 'tp', [(dev, dev ^ hop) for dev in range(8)])]
  transfers between devices with their start and end apart: 4 -> 7, of which waited for: 3 -> 6; matrix products, arithmetic and copies ran while one was open for 15% -> 15% of each run, Pallas kernels for 0% -> 0%
where the time goes in v1:
time: 278 us; the launch traced here: 277 us
  waiting for transfers between devices  111 us (40%)
  blocking collectives  64.7 us (23%)
  local copies, waits for them, and re-layouts  32.4 us (12%)
  matrix products  26.8 us (10%)
  other arithmetic  18.3 us (7%)
  between operations  13.4 us (5%)
  starting transfers between devices  9.67 us (3%)
    all_to_all x1, blocking collectives, local(): lax.all_to_all(outgoing, ('ep', 'tp'), split_axis=0, concat_axis=0, tiled...  64.7 us
    all_to_all x1, waiting for transfers between devices, local(): lax.all_to_all(outbound.reshape(expert_groups * width_groups, width_group...  51.6 us
    all_gather x3, waiting for transfers between devices, taken_in(): lax.all_gather(a, axis, axis=dim, tiled=True)  50.8 us
    gather x1, local copies, waits for them, and re-layouts, local(): picked = returned[row_index.reshape(-1)].astype(jnp.float32)  15.7 us
    dot_general x1, matrix products, add_hidden(): jnp.dot(arrived_rows, pieces[0][0], preferred_element_type=jnp.float32)  10.1 us
    dot_general x1, matrix products, add_hidden(): jnp.dot(arrived_rows, pieces[1][0], preferred_element_type=jnp.float32)  9.88 us
    another operation x2, other arithmetic  9.2 us
    all_to_all x1, starting transfers between devices, local(): lax.all_to_all(outbound.reshape(expert_groups * width_groups, width_group...  8.29 us
  transfers between devices with their start and end apart: 7, of which 6 were waited for; matrix products, arithmetic and copies ran while one was open for 15% of the time, Pallas kernels for 0%

profile of v1, /device:TPU:1, one launch (start us, length us, event | category | flops | bytes accessed | tf_op | source)
XLA Modules:
  0.0 276.7 jit_solution(16185036298853536639)
XLA Ops:
  6.5 0.0 copy-start
  6.5 0.0 copy-start.3
  6.5 0.0 all-gather.6.cloned.1.call-start
  6.5 0.7 all-gather.6.cloned.1.call-update
  7.3 0.0 all-gather.4.cloned.1.call-start
  7.3 0.7 all-gather.4.cloned.1.call-update
  8.0 0.0 all-gather.8.cloned.1.call-start
  8.1 0.7 all-gather.8.cloned.1.call-update
  8.7 0.9 copy.11
  9.7 0.3 eq.28
  10.0 0.3 reshape.220
  10.3 9.1 %reduce-window.6 = s32[8,16,4,128]{3,1,2,0:T(8,128)S(1)} reduce-window(s32[8,16,4,128]{3,1,2,0:T(8,128)S(1)} %fusion.21, s32[]{:T(128)} %constant.77.clone.1), window={size=1x1x1x128 pad=0_0x0_0x0_0x127_0}, to_apply=%region_1.0 | reduce-window | flops 8323072 | bytes 524292 | tf_op jit(solution)/shard_map/reduce-window
  19.4 0.1 slice.12
  19.5 0.3 copy.13
  19.8 0.1 fusion.23
  19.9 0.0 copy-done
  19.9 0.2 fusion.15
  20.1 0.0 copy-done.3
  20.1 0.2 fusion.17
  20.4 0.1 fusion.20
  20.6 2.4 scatter_custom_fusion
  23.0 6.0 %gather_fusion = bf16[1024,2048]{1,0:T(8,128)(2,1)} fusion(bf16[129,2048]{1,0:T(8,128)(2,1)S(1)} %concatenate.3, s32[1024]{0:T(1024)S(1)} %fusion.25), kind=kCustom, calls=%fused_computation | custom fusion | bytes 8392704 | tf_op jit(solution)/shard_map/gather | solution.py:53
  29.1 64.7 %all_to_all.10 = bf16[128,8,2048]{2,1,0:T(8,128)(2,1)} all-to-all(bf16[128,8,2048]{2,1,0:T(8,128)(2,1)} %bitcast.62), channel_id=1, replica_groups=mesh['ep'=16,'tp'=8] {'ep','tp'}, dimensions={0} | all-to-all | bytes 8388608 | tf_op jit(solution)/shard_map/all_to_all | solution.py:54
  93.7 0.0 all-gather.6.cloned.1.call-done
  93.7 9.9 %fusion.2 = f32[1024,1024]{1,0:T(8,128)} fusion(bf16[1,2048,1024]{2,1,0:T(8,128)(2,1)} %all-gather.6.cloned.1.call-done, bf16[128,8,2048]{2,1,0:T(8,128)(2,1)} %all_to_all.10), kind=kOutput, calls=%fused_computation.5 | convolution fusion | flops 4294967296 | bytes 12582912 | tf_op jit(solution)/shard_map/dot_general | solution.py:62
  103.6 26.1 %all-gather.4.cloned.1.call-done = bf16[1,2048,1024]{2,1,0:T(8,128)(2,1)} async-done(((bf16[1,2048,128]{2,1,0:T(8,128)(2,1)}), bf16[1,2048,1024]{2,1,0:T(8,128)(2,1)}) %all-gather.4.cloned.1.call-update) | async-done | bytes 4194320 | tf_op jit(solution)/shard_map/all_gather | solution.py:12
  129.7 10.1 %multiply_convert_fusion = bf16[1024,1024]{1,0:T(8,128)(2,1)S(1)} fusion(f32[1024,1024]{1,0:T(8,128)} %fusion.2, bf16[1,2048,1024]{2,1,0:T(8,128)(2,1)} %all-gather.4.cloned.1.call-done, bf16[128,8,2048]{2,1,0:T(8,128)(2,1)} %all_to_all.10), kind=kOutput, calls=%fused_computation.12 | convolution fusion | flops 4305453056 | bytes 14680064 | tf_op jit(solution)/shard_map/dot_general | solution.py:61
  139.8 24.7 %all-gather.8.cloned.1.call-done = bf16[1,1024,2048]{2,1,0:T(8,128)(2,1)} async-done(((bf16[1,128,2048]{2,1,0:T(8,128)(2,1)}), bf16[1,1024,2048]{2,1,0:T(8,128)(2,1)}) %all-gather.8.cloned.1.call-update) | async-done | bytes 4194320 | tf_op jit(solution)/shard_map/all_gather | solution.py:12
  164.5 6.9 %fusion.8 = bf16[1024,2048]{1,0:T(8,128)(2,1)S(1)} fusion(bf16[1024,1024]{1,0:T(8,128)(2,1)S(1)} %multiply_convert_fusion, bf16[1,1024,2048]{2,1,0:T(8,128)(2,1)} %all-gather.8.cloned.1.call-done), kind=kOutput, calls=%fused_computation.13 | convolution fusion | flops 4297064448 | bytes 10485760 | tf_op jit(solution)/shard_map/dot_general | solution.py:70
  171.3 2.6 copy.16
  173.9 0.0 copy-start.1
  173.9 0.0 copy-start.2
  173.9 8.3 %all-to-all-start.1 = ((bf16[128,8,8,256]{3,2,1,0:T(8,128)(2,1)}), bf16[128,8,8,256]{3,2,1,0:T(8,128)(2,1)}, u32[]{:S(2)}, u32[]{:S(2)}) async-start(bf16[128,8,8,256]{3,2,1,0:T(8,128)(2,1)} %bitcast.63), calls=%async_computation.1 | async-start | bytes 8388608 | tf_op jit(solution)/shard_map/all_to_all | solution.py:76
  182.2 0.0 copy-done.1
  182.3 0.2 copy.17
  182.5 0.3 mul.125
  182.9 0.0 copy-done.2
  182.9 0.2 copy.10
  183.1 0.2 compare_select_fusion
  183.3 51.6 %all-to-all-done.1 = bf16[128,8,8,256]{3,2,1,0:T(8,128)(2,1)} async-done(((bf16[128,8,8,256]{3,2,1,0:T(8,128)(2,1)}), bf16[128,8,8,256]{3,2,1,0:T(8,128)(2,1)}, u32[]{:S(2)}, u32[]{:S(2)}) %all-to-all-start.1) | async-done | bytes 4194336 | tf_op jit(solution)/shard_map/all_to_all | solution.py:76
  234.9 15.7 %gather_fusion.1 = bf16[4096,256]{1,0:T(8,128)(2,1)S(1)} fusion(bf16[8192,256]{1,0:T(8,128)(2,1)} %bitcast.12, s32[4096]{0:T(1024)S(1)} %broadcast_clamp_fusion), kind=kCustom, calls=%fused_computation.1 | custom fusion | bytes 4210688 | tf_op jit(solution)/shard_map/gather | solution.py:90
  250.6 2.9 %reshape.227 = f32[1024,4,256]{2,1,0:T(4,128)} reshape(bf16[4096,256]{1,0:T(8,128)(2,1)S(1)} %gather_fusion.1) | data formatting | bytes 6291456 | tf_op jit(solution)/shard_map/convert_element_type | solution.py:90
  253.5 0.0 copy-start.4
  253.5 7.2 %multiply_reduce_fusion = f32[1024,256]{1,0:T(8,128)S(1)} fusion(f32[1024,4,256]{2,1,0:T(4,128)} %reshape.227, f32[1024,4]{1,0:T(8,128)S(1)} %copy.10), kind=kLoop, calls=%fused_computation.11 | loop fusion | flops 1835008 | bytes 5259264 | tf_op jit(solution)/shard_map/reduce_sum | solution.py:92
  260.7 0.2 multiply_reduce_fusion.1
  260.9 1.0 collective-permute-start
  261.9 0.8 collective-permute-done
  262.7 0.2 collective-permute-start.1
  262.9 2.3 collective-permute-done.1
  265.2 0.1 collective-permute-start.2
  265.3 3.9 %collective-permute-done.2 = f32[1024]{0:T(1024)S(1)} collective-permute-done((f32[1024]{0:T(1024)S(1)}, f32[1024]{0:T(1024)S(1)}, u32[]{:S(2)}, u32[]{:S(2)}) %collective-permute-start.2) | collective-permute-done | bytes 4128 | tf_op jit(solution)/shard_map/ppermute | solution.py:96
  269.2 0.0 copy-done.4
  269.2 1.0 multiply_convert_fusion.1
  (16 shorter events, 0.2 us)
Async XLA Ops:
  6.5 13.4 %copy-start = (bf16[128,2048]{1,0:T(8,128)(2,1)S(1)}, bf16[128,2048]{1,0:T(8,128)(2,1)}, u32[]{:S(2)}) copy-start(bf16[128,2048]{1,0:T(8,128)(2,1)} %param.8) | copy-start | bytes 1572868
  6.5 13.6 %copy-start.3 = (f32[2048]{0:T(1024)S(1)}, f32[2048]{0:T(1024)}, u32[]{:S(2)}) copy-start(f32[2048]{0:T(1024)} %param.11) | copy-start | bytes 24580
  6.5 87.2 %all-gather.6.cloned.1.call-start = ((), (), s32[]{:S(2)}) async-start(), calls=%async_computation.3 | async-start | bytes 4718592 | tf_op jit(solution)/shard_map/all_gather | solution.py:12
  7.3 122.5 %all-gather.4.cloned.1.call-start = ((), (), s32[]{:S(2)}) async-start(), calls=%async_computation.2 | async-start | bytes 4718592 | tf_op jit(solution)/shard_map/all_gather | solution.py:12
  8.0 156.4 %all-gather.8.cloned.1.call-start = ((), (), s32[]{:S(2)}) async-start(), calls=%async_computation.4 | async-start | bytes 4718592 | tf_op jit(solution)/shard_map/all_gather | solution.py:12
  173.9 8.3 %copy-start.1 = (s32[1024,4]{0,1:T(4,128)S(1)}, s32[1024,4]{0,1:T(4,128)}, u32[]{:S(2)}) copy-start(s32[1024,4]{0,1:T(4,128)} %param.9) | copy-start | bytes 49156
  173.9 9.0 %copy-start.2 = (f32[1024,4]{0,1:T(4,128)S(1)}, f32[1024,4]{0,1:T(4,128)}, u32[]{:S(2)}) copy-start(f32[1024,4]{0,1:T(4,128)} %param.10) | copy-start | bytes 49156
  173.9 61.0 %all-to-all-start.1 = ((bf16[128,8,8,256]{3,2,1,0:T(8,128)(2,1)}), bf16[128,8,8,256]{3,2,1,0:T(8,128)(2,1)}, u32[]{:S(2)}, u32[]{:S(2)}) async-start(bf16[128,8,8,256]{3,2,1,0:T(8,128)(2,1)} %bitcast.63), calls=%async_computation.1 | async-start | bytes 8388608 | tf_op jit(solution)/shard_map/all_to_all | solution.py:76
  253.5 15.7 %copy-start.4 = (f32[256]{0:T(256)S(1)}, f32[256]{0:T(256)}, u32[]{:S(2)}) copy-start(f32[256]{0:T(256)} %param.15) | copy-start | bytes 3076
  260.9 1.8 collective-permute-start
  262.7 2.5 collective-permute-start.1
  265.2 4.0 %collective-permute-start.2 = (f32[1024]{0:T(1024)S(1)}, f32[1024]{0:T(1024)S(1)}, u32[]{:S(2)}, u32[]{:S(2)}) collective-permute-start(f32[1024]{0:T(1024)S(1)} %add.168), channel_id=1, source_target_pairs={{0,4},{1,5},{2,6},{3,7},{4,0},{5,1},{6,2},{7,3},{8,12},{9,13},{10,... | collective-permute-start | bytes 12296 | tf_op jit(solution)/shard_map/ppermute | solution.py:96
Sparse Core Ops, SparseCore 0:
  9.0 63.1 all-gather.5
  73.9 55.8 all-gather.3
  131.4 32.9 all-gather.7
